TPU v7x, 32 devices: a whole 2x2x4 slice. The times are simulated.
32 devices in a mesh: sp: 4 (over z), fs: 4 (over y, x), tp: 2 (over core).
Axes of the slice: x: 2, y: 2, z: 4, core: 2. Of those that a mesh axis runs over, the one named last changes fastest.
Arguments:
- hidden_in: bfloat16 [4, 1024, 2048], P('fs', 'sp', 'tp'), may hold values from -6 to 6
- sb_query_w: bfloat16 [2048, 1024], P('fs', 'tp'), may hold values from -0.21875 to 0.21875
- sb_key_w: bfloat16 [2048, 1024], P('fs', 'tp'), may hold values from -0.21875 to 0.21875
- sb_value_w: bfloat16 [2048, 1024], P('fs', 'tp'), may hold values from -0.125 to 0.125
- sb_offset: float32 [16], P('tp'), may hold values from -16 to -6
- delta_query_w: bfloat16 [2048, 1024], P('fs', 'tp'), may hold values from -0.125 to 0.125
- delta_key_w: bfloat16 [2048, 1024], P('fs', 'tp'), may hold values from -0.125 to 0.125
- delta_value_w: bfloat16 [2048, 1024], P('fs', 'tp'), may hold values from -0.125 to 0.125
- decay_w: bfloat16 [2048, 8], P(None, 'tp'), may hold values from -0.125 to 0.125
- write_w: bfloat16 [2048, 8], P(None, 'tp'), may hold values from -0.125 to 0.125
- write_bias: float32 [8], P('tp'), may hold values from -7 to 1.5
- decay_log_scale: float32 [8], P('tp'), may hold values from -14 to -3
- decay_shift: float32 [4, 8, 1024], P('fs', 'tp', 'sp'), may hold values from -3 to 0
- head_gain: float32 [128], replicated, may hold values from 0.1 to 1.9
- sb_out_w: bfloat16 [1024, 2048], P('tp'), may hold values from -0.125 to 0.125
- delta_out_w: bfloat16 [1024, 2048], P('tp'), may hold values from -0.125 to 0.125
Outputs:
- mixed_out: bfloat16 [4, 1024, 2048], P('fs', ('sp', 'tp'))
All inputs are finite; a program needn't handle non-finite values.
Results may differ from a plain program's by a relative error of at most 0.015.
Values may be sent and summed in bfloat16 or wider, within the bound.
A program may use at most 128 MiB of HBM per device.

v0:
```python
import jax
import jax.numpy as jnp
from jax import lax
from jax.sharding import PartitionSpec as P

SB_DIM = 64
GDN_DIM = 128
BLOCK = 64
EXACT_MATMUL = lax.Precision.HIGHEST
NORM_EPS = 1e-06


def carried_in(value, axis, combine, identity):
    devices, index = (lax.axis_size(axis), lax.axis_index(axis))
    everything = jax.tree.map(
        lambda part, kind: lax.all_gather(part.astype(kind), axis),
        value,
        (jnp.bfloat16, jnp.bfloat16),
    )
    start = jax.tree.map(
        lambda part, zero: jnp.broadcast_to(jnp.asarray(zero, part.dtype), part.shape),
        value,
        identity,
    )

    def lap(k, before):
        reached = k < index
        new = combine(
            before, jax.tree.map(lambda part, own: part[k].astype(own.dtype), everything, value)
        )
        return jax.tree.map(lambda a, b: jnp.where(reached, a, b), new, before)

    return lax.fori_loop(0, devices, lap, start)


def unit_lower_inverse(strict_part):
    order_size = strict_part.shape[-1]
    powered = strict_part
    inverse = jnp.eye(order_size, dtype=strict_part.dtype) - strict_part
    for repeat_number in range(max(1, (order_size - 1).bit_length()) - 1):
        powered = jnp.einsum("...ij,...jk->...ik", powered, powered, precision=EXACT_MATMUL)
        inverse = inverse + jnp.einsum(
            "...ij,...jk->...ik", inverse, powered, precision=EXACT_MATMUL
        )
    return inverse


def to_blocks(row_data, block_span):
    blocks_count = row_data.shape[0] // block_span
    shaped = row_data.reshape((blocks_count, block_span) + row_data.shape[1:])
    return jnp.swapaxes(shaped, 1, 2)


def from_blocks(blocked):
    swapped = jnp.swapaxes(blocked, 1, 2)
    return swapped.reshape((-1,) + swapped.shape[2:])


def unit_rows(vectors):
    return vectors * lax.rsqrt(jnp.sum(vectors * vectors, axis=-1, keepdims=True) + NORM_EPS)


def delta_inputs(
    query_proj,
    key_proj,
    value_proj,
    decay_pre,
    write_pre,
    write_bias,
    decay_log_scale,
    shift_rows,
    head_count,
    head_size,
):
    query_act = jax.nn.silu(query_proj.astype(jnp.float32)).reshape(-1, head_count, head_size)
    key_act = jax.nn.silu(key_proj.astype(jnp.float32)).reshape(-1, head_count, head_size)
    value_rows = jax.nn.silu(value_proj.astype(jnp.float32)).reshape(-1, head_count, head_size)
    queries = unit_rows(query_act) * head_size ** (-0.5)
    key_rows = unit_rows(key_act)
    log_decay = -jnp.exp(decay_log_scale) * jax.nn.softplus(decay_pre) + shift_rows
    strength = jax.nn.sigmoid(write_pre + write_bias)
    return (queries, key_rows, value_rows, log_decay, strength)


def delta_prepare(queries, key_rows, value_rows, log_decay, strength):
    block_span = queries.shape[2]
    cumulative = jnp.cumsum(log_decay, axis=-1)
    row_place = lax.broadcasted_iota(jnp.int32, (block_span, block_span), 0)
    col_place = lax.broadcasted_iota(jnp.int32, (block_span, block_span), 1)
    inclusive = col_place <= row_place
    strictly = col_place < row_place
    spread = cumulative[..., :, None] - cumulative[..., None, :]
    decay_table = jnp.where(inclusive, jnp.exp(jnp.where(inclusive, spread, 0.0)), 0.0)
    keys_beta = key_rows * strength[..., None]
    lower_part = jnp.where(
        strictly,
        jnp.einsum("nhik,nhjk->nhij", keys_beta, key_rows, precision=EXACT_MATMUL) * decay_table,
        0.0,
    )
    inverse = unit_lower_inverse(lower_part)
    growth = jnp.exp(cumulative)
    state_updates = jnp.einsum(
        "nhij,nhjv->nhiv", inverse, value_rows * strength[..., None], precision=EXACT_MATMUL
    )
    erase_term = jnp.einsum(
        "nhij,nhjk->nhik", inverse, keys_beta * growth[..., None], precision=EXACT_MATMUL
    )
    inside_block = (
        jnp.einsum("nhik,nhjk->nhij", queries, key_rows, precision=EXACT_MATMUL) * decay_table
    )
    boosted_query = queries * growth[..., None]
    damped_keys = key_rows * jnp.exp(cumulative[..., -1:] - cumulative)[..., None]
    decay_per_block = jnp.exp(cumulative[..., -1])
    return (state_updates, erase_term, inside_block, boosted_query, damped_keys, decay_per_block)


def delta_step(memory_state, inputs):
    state_updates, erase_term, inside_block, boosted_query, damped_keys, decay_per_block = inputs
    fixed_values = state_updates - jnp.einsum(
        "mzq,mqc->mzc", erase_term, memory_state, precision=EXACT_MATMUL
    )
    produced_rows = jnp.einsum(
        "mzq,mqc->mzc", boosted_query, memory_state, precision=EXACT_MATMUL
    ) + jnp.einsum("efq,eqn->efn", inside_block, fixed_values, precision=EXACT_MATMUL)
    memory_state = memory_state * decay_per_block[:, None, None] + jnp.einsum(
        "wam,waz->wmz", damped_keys, fixed_values, precision=EXACT_MATMUL
    )
    return (memory_state, produced_rows)


def transition_step(carried, inputs):
    memory_state, transfer = carried
    state_updates, erase_term, inside_block, boosted_query, damped_keys, decay_per_block = inputs
    fixed_values = state_updates - jnp.einsum(
        "mzq,mqc->mzc", erase_term, memory_state, precision=EXACT_MATMUL
    )
    coupling = jnp.einsum("hik,hil->hkl", damped_keys, erase_term, precision=EXACT_MATMUL)
    memory_state = memory_state * decay_per_block[:, None, None] + jnp.einsum(
        "wam,waz->wmz", damped_keys, fixed_values, precision=EXACT_MATMUL
    )
    transfer = transfer * decay_per_block[:, None, None] - jnp.einsum(
        "hkl,hlm->hkm", coupling, transfer, precision=EXACT_MATMUL
    )
    return ((memory_state, transfer), None)


def compose(prior_blocks, following_blocks):
    joined_map = jnp.einsum(
        "hkl,hlm->hkm", following_blocks[0], prior_blocks[0], precision=EXACT_MATMUL
    )
    joined_state = (
        jnp.einsum("djo,dog->djg", following_blocks[0], prior_blocks[1], precision=EXACT_MATMUL)
        + following_blocks[1]
    )
    return (joined_map, joined_state)


def stick_block(queries, key_rows, value_rows, query_place, key_place, offsets):
    scale_factor = queries.shape[-1] ** (-0.5)
    scores = (
        jnp.einsum("qhd,khd->hqk", queries, key_rows, preferred_element_type=jnp.float32)
        * scale_factor
        + offsets[:, None, None]
    )
    visible = key_place[None, :] < query_place[:, None]
    skipped = jnp.where(visible, jax.nn.log_sigmoid(-scores), 0.0)
    beyond = lax.cumsum(skipped, axis=2, reverse=True) - skipped
    weights = jnp.where(visible, jnp.exp(jax.nn.log_sigmoid(scores) + beyond), 0.0).astype(
        jnp.bfloat16
    )
    partial_value = jnp.einsum(
        "hqk,khd->qhd", weights, value_rows, preferred_element_type=jnp.float32
    )
    return (partial_value, jnp.sum(skipped, axis=2).T)


def stick_combine(partials, totals):
    beyond = jnp.cumsum(totals[::-1], axis=0)[::-1] - totals
    return jnp.sum(partials * jnp.exp(beyond)[..., None], axis=0)


def on_device(
    hidden_in,
    sb_query_w,
    sb_key_w,
    sb_value_w,
    sb_offset,
    delta_query_w,
    delta_key_w,
    delta_value_w,
    decay_w,
    write_w,
    write_bias,
    decay_log_scale,
    decay_shift,
    head_gain,
    sb_out_w,
    delta_out_w,
):
    token_rows = hidden_in.shape[1]
    local_in = hidden_in.reshape(token_rows, hidden_in.shape[2])
    gathered = (
        lax.all_gather(sb_query_w, "fs", axis=0, tiled=True),
        lax.all_gather(sb_key_w, "fs", axis=0, tiled=True),
        lax.all_gather(sb_value_w, "fs", axis=0, tiled=True),
        lax.all_gather(delta_query_w, "fs", axis=0, tiled=True),
        lax.all_gather(delta_key_w, "fs", axis=0, tiled=True),
        lax.all_gather(delta_value_w, "fs", axis=0, tiled=True),
    )
    in_weights = tuple(gathered) + (decay_w, write_w)
    portion = lax.all_gather(local_in, "tp", axis=1, tiled=True)
    projected = tuple(
        (jnp.dot(portion, weight, preferred_element_type=jnp.float32) for weight in in_weights)
    )
    sb_heads = sb_offset.shape[0]
    delta_heads = decay_log_scale.shape[0]
    sb_query = projected[0].astype(jnp.bfloat16).reshape(token_rows, sb_heads, SB_DIM)
    sb_keys = projected[1].astype(jnp.bfloat16)
    sb_values = projected[2].astype(jnp.bfloat16)
    shift_rows = decay_shift.reshape(delta_heads, token_rows).T
    queries, key_rows, value_rows, log_decay, strength = delta_inputs(
        projected[3].astype(jnp.bfloat16),
        projected[4].astype(jnp.bfloat16),
        projected[5].astype(jnp.bfloat16),
        projected[6],
        projected[7],
        write_bias,
        decay_log_scale,
        shift_rows,
        delta_heads,
        GDN_DIM,
    )
    prepared = delta_prepare(
        to_blocks(queries, BLOCK),
        to_blocks(key_rows, BLOCK),
        to_blocks(value_rows, BLOCK),
        to_blocks(log_decay, BLOCK),
        to_blocks(strength, BLOCK),
    )
    identity_map = jnp.broadcast_to(
        jnp.eye(GDN_DIM, dtype=jnp.float32), (delta_heads, GDN_DIM, GDN_DIM)
    )
    empty_state = jnp.zeros((delta_heads, GDN_DIM, GDN_DIM), jnp.float32)
    (local_end, local_map), unused_out = lax.scan(
        transition_step, (empty_state, identity_map), prepared
    )
    own_first = lax.axis_index("sp") * token_rows
    query_place = own_first + lax.iota(jnp.int32, token_rows)
    sp_count = lax.axis_size("sp")
    slot_out = jnp.zeros((sp_count, token_rows, sb_heads, SB_DIM), jnp.float32)
    slot_total = jnp.zeros((sp_count, token_rows, sb_heads), jnp.float32)

    def absorb(slot_arrays, address_portion, value_part, shard_first):

        def active(current):
            partial_value, totals = stick_block(
                sb_query,
                address_portion.reshape(token_rows, sb_heads, SB_DIM),
                value_part.reshape(token_rows, sb_heads, SB_DIM),
                query_place,
                shard_first + lax.iota(jnp.int32, token_rows),
                sb_offset,
            )
            slot_index = shard_first // token_rows
            return (
                lax.dynamic_update_index_in_dim(current[0], partial_value, slot_index, 0),
                lax.dynamic_update_index_in_dim(current[1], totals, slot_index, 0),
            )

        def inactive(current):
            return current

        usable = jnp.logical_and(shard_first >= 0, shard_first <= own_first)
        return lax.cond(usable, active, inactive, slot_arrays)

    key_block = lax.all_gather(sb_keys, "sp", axis=0, tiled=True)
    value_block = lax.all_gather(sb_values, "sp", axis=0, tiled=True)

    def per_shard(shard_number, current):
        row_begin = shard_number * token_rows
        return absorb(
            current,
            lax.dynamic_slice_in_dim(key_block, row_begin, token_rows, 0),
            lax.dynamic_slice_in_dim(value_block, row_begin, token_rows, 0),
            row_begin,
        )

    slot_arrays = lax.fori_loop(
        0, key_block.shape[0] // token_rows, per_shard, (slot_out, slot_total)
    )
    unused_map, incoming = carried_in(
        (local_map, local_end), "sp", compose, (identity_map, empty_state)
    )
    sb_mixed = (
        stick_combine(slot_arrays[0], slot_arrays[1])
        .astype(jnp.bfloat16)
        .reshape(token_rows, sb_heads * SB_DIM)
    )
    unused_end, produced_rows = lax.scan(delta_step, incoming, prepared)
    produced_rows = from_blocks(produced_rows)
    normed = (
        produced_rows
        * lax.rsqrt(jnp.mean(produced_rows * produced_rows, axis=-1, keepdims=True) + NORM_EPS)
        * head_gain
    )
    delta_mixed = normed.astype(jnp.bfloat16).reshape(token_rows, delta_heads * GDN_DIM)
    result = lax.psum_scatter(
        (
            jnp.dot(sb_mixed, sb_out_w, preferred_element_type=jnp.float32)
            + jnp.dot(delta_mixed, delta_out_w, preferred_element_type=jnp.float32)
        ).astype(jnp.bfloat16),
        "tp",
        scatter_dimension=0,
        tiled=True,
    ).astype(jnp.float32)
    return result.astype(jnp.bfloat16).reshape(1, result.shape[0], result.shape[1])


def solution(mesh):
    return jax.shard_map(
        on_device,
        mesh=mesh,
        in_specs=(
            P("fs", "sp", "tp"),
            P("fs", "tp"),
            P("fs", "tp"),
            P("fs", "tp"),
            P("tp"),
            P("fs", "tp"),
            P("fs", "tp"),
            P("fs", "tp"),
            P(None, "tp"),
            P(None, "tp"),
            P("tp"),
            P("tp"),
            P("fs", "tp", "sp"),
            P(),
            P("tp", None),
            P("tp", None),
        ),
        out_specs=P("fs", ("sp", "tp"), None),
        check_vma=False,
    )
```

profile of v0, /device:TPU:0, one launch (start us, length us, event | category | flops | bytes accessed | tf_op | source)
XLA Modules:
  0.0 387.4 jit_solution(17021583337816945138)
XLA Ops:
  12.1 8.6 %all-gather.29.cloned.1.call-done = bf16[1,256,2048]{2,1,0:T(8,128)(2,1)} async-done(((bf16[1,256,1024]{2,1,0:T(8,128)(2,1)}), bf16[1,256,2048]{2,1,0:T(8,128)(2,1)}) %all-gather.29.cloned.1.call-update) | async-done | bytes 1048592 | tf_op jit(solution)/shard_map/all_gather | solution.py:211
  20.7 1.6 fusion.111
  23.6 1.6 fusion.67
  25.4 33.6 %all-gather.23.cloned.1.call-done = bf16[2048,512]{1,0:T(8,128)(2,1)} async-done(((bf16[512,512]{1,0:T(8,128)(2,1)}), bf16[2048,512]{1,0:T(8,128)(2,1)}) %all-gather.23.cloned.1.call-update) | async-done | bytes 2097168 | tf_op jit(solution)/shard_map/all_gather | solution.py:207
  58.9 3.7 fusion.116
  65.5 1.3 fusion.60
  71.4 1.4 fusion.124
  72.9 1.4 convolution_add_fusion.6
  74.3 21.7 %all-gather.25.cloned.1.call-done = bf16[2048,512]{1,0:T(8,128)(2,1)} async-done(((bf16[512,512]{1,0:T(8,128)(2,1)}), bf16[2048,512]{1,0:T(8,128)(2,1)}) %all-gather.25.cloned.1.call-update) | async-done | bytes 2097168 | tf_op jit(solution)/shard_map/all_gather | solution.py:208
  96.0 3.5 divide_multiply_fusion.1
  99.5 2.0 reshape_reshape.3
  101.5 1.9 convolution_add_fusion.5
  103.5 2.1 fusion.78
  105.6 1.6 fusion.82
  107.1 25.7 %all-gather.27.cloned.1.call-done = bf16[2048,512]{1,0:T(8,128)(2,1)} async-done(((bf16[512,512]{1,0:T(8,128)(2,1)}), bf16[2048,512]{1,0:T(8,128)(2,1)}) %all-gather.27.cloned.1.call-update) | async-done | bytes 2097168 | tf_op jit(solution)/shard_map/all_gather | solution.py:206
  132.9 3.8 fusion.117
  136.7 2.0 mul.197
  138.7 1.4 reduce_sum.50
  140.3 2.1 reshape.155
  142.3 2.9 bitcast_multiply_fusion.1
  145.3 19.1 %while.57 = (s32[]{:T(128)}, f32[4,128,128]{2,1,0:T(8,128)S(1)}, f32[4,128,128]{2,1,0:T(8,128)S(1)}, f32[4,4]{1,0:T(4,128)S(1)}, f32[4,4,64,128]{3,2,1,0:T(8,128...) while((s32[]{:T(128)}, f32[4,128,128]{2,1,0:T(8,128)S(1)}, ...), condition=%wide.region_12.13_spmd.clone, body=%wide.region_11.12_spmd.clone.sunk | while | flops 252084224 | bytes 3279532 | solution.py:244
  145.3 1.3 convolution_subtract_fusion.7
  146.6 1.5 convolution_add_fusion.14
  148.1 1.5 fusion.213
  151.3 1.5 convolution_add_fusion.14
  152.8 1.5 fusion.213
  156.1 1.5 convolution_add_fusion.14
  157.6 1.5 fusion.213
  160.9 1.5 convolution_add_fusion.14
  162.4 1.5 fusion.213
  165.0 16.0 %all-gather.1 = bf16[16,128,128]{2,1,0:T(8,128)(2,1)} all-gather(bf16[4,128,128]{2,1,0:T(8,128)(2,1)S(1)} %convert_element_type.96), channel_id=3, replica_groups=mesh['sp'=4,'fs'=4,'tp'=2] {'sp'}, dimensions={0}, use_global_device_ids=true | all-gather | bytes 655360 | tf_op jit(solution)/shard_map/all_gather | solution.py:16
  180.9 3.4 convolution_convert_fusion.5
  184.4 17.0 %all-gather.2 = bf16[16,128,128]{2,1,0:T(8,128)(2,1)} all-gather(bf16[4,128,128]{2,1,0:T(8,128)(2,1)S(1)} %convert_element_type.97), channel_id=4, replica_groups=mesh['sp'=4,'fs'=4,'tp'=2] {'sp'}, dimensions={0}, use_global_device_ids=true | all-gather | bytes 655360 | tf_op jit(solution)/shard_map/all_gather | solution.py:16
  201.4 3.0 convolution_multiply_fusion
  204.5 2.2 all-gather.19.cloned.1.call-done
  206.7 3.3 convolution_convert_fusion.3
  210.0 5.3 %while.58 = (s32[]{:T(128)}, f32[4,128,128]{2,1,0:T(8,128)S(1)}, s32[]{:T(128)}, bf16[4,4,128,128]{3,2,1,0:T(8,128)(2,1)}, bf16[4,4,128,128]{3,2,1,0:T(8,128)(2,1)}, /*index=5*/s32[]{:T(128)}, s32[]{:T(128)}) while((s32[]{:T(128)}, f32[4,128,128]{2,1,0:T(8,128)S(1)}, s32[]{:T(128)}, bf16[4,4,128,128]{3,2,1,0:T(8,128)(2,1)}, ...), condition=%wide.region_14.15_spmd.clone, body=%wide.region_13.14_spmd.clone.sunk | while | flops 100990976 | bytes 1575519 | solution.py:33
  210.0 1.3 fusion.216
  214.1 1.3 fusion.216
  215.4 23.9 %while.56 = (s32[]{:T(128)}, f32[4,128,128]{2,1,0:T(8,128)S(1)}, f32[4,4,64,128]{3,2,1,0:T(8,128)S(1)}, f32[4,4]{1,0:T(4,128)}, f32[4,4,64,128]{3,2,1,0:T(8,128)...) while((s32[]{:T(128)}, f32[4,128,128]{2,1,0:T(8,128)S(1)}, ...), condition=%wide.region_17.18_spmd, body=%wide.region_16.17_spmd.sunk | while | flops 176357376 | bytes 2493593 | solution.py:299
  215.5 1.3 convolution_subtract_fusion.6
  217.9 1.3 fusion.203
  219.9 1.5 convolution_add_fusion.13
  221.4 1.3 convolution_subtract_fusion.6
  225.8 1.5 convolution_add_fusion.13
  229.8 1.3 fusion.203
  231.8 1.5 convolution_add_fusion.13
  235.8 1.3 fusion.203
  237.8 1.5 convolution_add_fusion.13
  240.8 2.9 all-gather.17.cloned.1.call-done
  243.7 2.6 convolution_convert_fusion.4
  247.2 26.1 %all-gather.15.cloned.1.call-done = bf16[1024,512]{1,0:T(8,128)(2,1)} async-done(((bf16[256,512]{1,0:T(8,128)(2,1)}), bf16[1024,512]{1,0:T(8,128)(2,1)}) %all-gather.15.cloned.1.call-update) | async-done | bytes 1048592 | tf_op jit(solution)/shard_map/all_gather | solution.py:276
  273.3 2.3 copy.80
  275.6 26.7 %all-gather.21.cloned.1.call-done = bf16[1024,512]{1,0:T(8,128)(2,1)} async-done(((bf16[256,512]{1,0:T(8,128)(2,1)}), bf16[1024,512]{1,0:T(8,128)(2,1)}) %all-gather.21.cloned.1.call-update) | async-done | bytes 1048592 | tf_op jit(solution)/shard_map/all_gather | solution.py:277
  302.3 2.3 copy.81
  304.6 1.6 broadcast_in_dim.81
  306.8 14.7 %while.59 = (s32[]{:T(128)}, f32[4,256,8,64]{1,3,2,0:T(8,128)}, f32[4,256,8]{1,2,0:T(8,128)}, s32[]{:T(128)}, bf16[1024,512]{0,1:T(8,128)(2,1)}, /*index=5*/bf16...) while((s32[]{:T(128)}, f32[4,256,8,64]{1,3,2,0:T(8,128)}, ...), condition=%wide.region_6.7_spmd.clone.clone, body=%wide.region_0.6_spmd.clone.clone.sunk | while | flops 218698256 | bytes 25745960 | solution.py:288
  306.8 14.7 %conditional.4 = ((f32[4,256,8,64]{1,3,2,0:T(8,128)}, f32[4,256,8]{1,2,0:T(8,128)})) conditional(s32[]{:T(128)} %convert_element_type.140, (f32[4,256,8,64]{1,3,2,0:T(8,128)}, f32[4,256,8]{1,2,0:T(8,128)}) %tuple.124, (s32[]{:T(128)}, s32[]{:T(128)}, bf16[1024,512]{0,1:T(8,128)(2,1)}, bf16[256,8,64]{0,2,1:T(8,128)(2,1)}, f32[8]{0:T(128)S(1)}, ...), branch_computations={%region_1.1_spmd, %region_2.0_spmd} | conditional | flops 218698256 | bytes 25744700 | solution.py:274
  308.0 2.7 fusion.17
  310.7 5.1 %fusion.13 = f32[8,256,2,128]{1,0,3,2:T(8,128)S(1)} fusion(f32[8,256,2,128]{1,3,2,0:T(8,128)S(1)} %bitcast.258), kind=kOutput, calls=%fused_computation.18 | output fusion | flops 66584576 | bytes 4194304 | tf_op jit(solution)/shard_map/reduce-window.6
  316.7 3.0 fusion.6
  323.2 1.8 multiply_reduce_fusion
  326.9 1.7 fusion.59
  328.6 51.9 %reduce-scatter.2.cloned.1.call-done = bf16[128,2048]{1,0:T(8,128)(2,1)} async-done(((bf16[256,2048]{1,0:T(8,128)(2,1)}), bf16[128,2048]{1,0:T(8,128)(2,1)}) %reduce-scatter.2.cloned.1.call-update) | async-done | bytes 524304 | tf_op jit(solution)/shard_map/reduce_scatter | solution.py:307
  (152 shorter events, 44.5 us)
Async XLA Ops:
  6.5 318.5 %copy-start = (bf16[512,2048]{1,0:T(8,128)(2,1)S(1)}, bf16[512,2048]{1,0:T(8,128)(2,1)}, u32[]{:S(2)}) copy-start(bf16[512,2048]{1,0:T(8,128)(2,1)} %param.40) | copy-start | bytes 6291460
  6.5 4.9 %copy-start.18 = (f32[4]{0:T(128)S(1)}, f32[4]{0:T(128)}, u32[]{:S(2)}) copy-start(f32[4]{0:T(128)} %param.37) | copy-start | bytes 52
  6.5 4.9 %copy-start.17 = (f32[128]{0:T(128)S(1)}, f32[128]{0:T(128)}, u32[]{:S(2)}) copy-start(f32[128]{0:T(128)} %param.39) | copy-start | bytes 1540
  6.5 14.1 %copy-start.9 = (bf16[2048,4]{0,1:T(4,128)(2,1)S(1)}, bf16[2048,4]{0,1:T(4,128)(2,1)}, u32[]{:S(2)}) copy-start(bf16[2048,4]{0,1:T(4,128)(2,1)} %param.34) | copy-start | bytes 49156
  6.5 14.1 %copy-start.14 = (f32[1,4,256]{2,1,0:T(4,128)S(1)}, f32[1,4,256]{2,1,0:T(4,128)}, u32[]{:S(2)}) copy-start(f32[1,4,256]{2,1,0:T(4,128)} %param.38) | copy-start | bytes 12292
  6.5 14.1 %all-gather.29.cloned.1.call-start = ((), (), s32[]{:S(2)}) async-start(), calls=%async_computation.10 | async-start | bytes 1572864 | tf_op jit(solution)/shard_map/all_gather | solution.py:211
  7.3 16.3 %copy-start.10 = (bf16[2048,4]{0,1:T(4,128)(2,1)S(1)}, bf16[2048,4]{0,1:T(4,128)(2,1)}, u32[]{:S(2)}) copy-start(bf16[2048,4]{0,1:T(4,128)(2,1)} %param.35) | copy-start | bytes 49156
  7.3 16.3 %copy-start.16 = (f32[4]{0:T(128)S(1)}, f32[4]{0:T(128)}, u32[]{:S(2)}) copy-start(f32[4]{0:T(128)} %param.36) | copy-start | bytes 52
  7.3 51.6 %all-gather.23.cloned.1.call-start = ((), (), s32[]{:S(2)}) async-start(), calls=%async_computation.6 | async-start | bytes 2621440 | tf_op jit(solution)/shard_map/all_gather | solution.py:207
  8.1 87.9 %all-gather.25.cloned.1.call-start = ((), (), s32[]{:S(2)}) async-start(), calls=%async_computation.7 | async-start | bytes 2621440 | tf_op jit(solution)/shard_map/all_gather | solution.py:208
  8.8 124.1 %all-gather.27.cloned.1.call-start = ((), (), s32[]{:S(2)}) async-start(), calls=%async_computation.8 | async-start | bytes 2621440 | tf_op jit(solution)/shard_map/all_gather | solution.py:206
  9.4 171.6 %all-gather.13.cloned.1.call-start = ((), (), s32[]{:S(2)}) async-start(), calls=%async_computation.1 | async-start | bytes 2621440 | tf_op jit(solution)/shard_map/all_gather | solution.py:204
  10.0 196.7 %all-gather.19.cloned.1.call-start = ((), (), s32[]{:S(2)}) async-start(), calls=%async_computation.4 | async-start | bytes 2621440 | tf_op jit(solution)/shard_map/all_gather | solution.py:205
  10.5 233.2 %all-gather.17.cloned.1.call-start = ((), (), s32[]{:S(2)}) async-start(), calls=%async_computation.3 | async-start | bytes 2621440 | tf_op jit(solution)/shard_map/all_gather | solution.py:203
  11.3 262.0 %all-gather.15.cloned.1.call-start = ((), (), s32[]{:S(2)}) async-start(), calls=%async_computation.2 | async-start | bytes 1310720 | tf_op jit(solution)/shard_map/all_gather | solution.py:276
  11.3 54.2 %copy-start.13 = (pred[64,64]{1,0:T(8,128)(4,1)}, pred[64,64]{1,0:T(8,128)(4,1)S(1)}, u32[]{:S(2)}) copy-start(pred[64,64]{1,0:T(8,128)(4,1)S(1)} %iota_compare_fusion.1) | copy-start | bytes 12292
  65.5 1.3 copy-start.1
  74.3 27.2 %copy-start.3 = (f32[4,4,64,64]{3,2,1,0:T(8,128)S(1)}, f32[4,4,64,64]{3,2,1,0:T(8,128)}, u32[]{:S(2)}) copy-start(f32[4,4,64,64]{3,2,1,0:T(8,128)} %fusion.124) | copy-start | bytes 786436
  101.5 4.0 %copy-start.5 = (f32[4,64,4,128]{3,2,1,0:T(4,128)S(1)}, f32[4,64,4,128]{3,2,1,0:T(4,128)}, u32[]{:S(2)}) copy-start(f32[4,64,4,128]{3,2,1,0:T(4,128)} %reshape_reshape.3) | copy-start | bytes 1572868
  140.3 5.0 %copy-start.8 = (f32[4,64,4]{1,2,0:T(4,128)}, f32[4,64,4]{1,2,0:T(4,128)S(1)}, u32[]{:S(2)}) copy-start(f32[4,64,4]{1,2,0:T(4,128)S(1)} %copy.89) | copy-start | bytes 12292
  164.4 0.6 copy-start.15
  180.9 20.5 %copy-start.2 = (f32[4,64,4,128]{3,2,1,0:T(4,128)S(1)}, f32[4,64,4,128]{3,2,1,0:T(4,128)}, u32[]{:S(2)}) copy-start(f32[4,64,4,128]{3,2,1,0:T(4,128)} %copy-done.1) | copy-start | bytes 1572868
  184.3 118.0 %all-gather.21.cloned.1.call-start = ((), (), s32[]{:S(2)}) async-start(), calls=%async_computation.5 | async-start | bytes 1310720 | tf_op jit(solution)/shard_map/all_gather | solution.py:277
  210.0 5.4 %copy-start.7 = (f32[4,4,64,128]{3,2,1,0:T(8,128)S(1)}, f32[4,4,64,128]{3,2,1,0:T(8,128)}, u32[]{:S(2)}) copy-start(f32[4,4,64,128]{3,2,1,0:T(8,128)} %custom-call.2) | copy-start | bytes 1572868
  215.4 165.2 %reduce-scatter.2.cloned.1.call-start = ((), (), s32[]{:S(2)}) async-start(), calls=%async_computation.9 | async-start | bytes 1572864 | tf_op jit(solution)/shard_map/reduce_scatter | solution.py:307
  275.6 31.2 %copy-start.11 = (f32[8]{0:T(128)S(1)}, f32[8]{0:T(128)}, u32[]{:S(2)}) copy-start(f32[8]{0:T(128)} %param.30) | copy-start | bytes 100
  325.1 1.1 copy-start.4
  325.1 1.8 copy-start.6
  325.1 1.8 copy-start.12
Sparse Core Ops, SparseCore 0:
  8.9 11.7 all-gather.28
  22.5 36.3 all-gather.22
  60.8 35.1 all-gather.24
  97.7 35.1 all-gather.26
  134.6 35.1 all-gather.12
  171.5 35.1 all-gather.18
  208.5 35.1 all-gather.16
  245.3 27.9 all-gather.14
  274.9 27.3 all-gather.20
  328.7 51.7 reduce-scatter.1
where the time goes:
time: 389 us; the launch traced here: 387 us
  waiting for transfers between devices  204 us (52%)
  matrix products  92.1 us (24%)
  blocking collectives  33 us (8%)
  local copies, waits for them, and re-layouts  26.2 us (7%)
  other arithmetic  17.2 us (4%)
  between operations  14 us (4%)
    reduce_scatter x1, waiting for transfers between devices, on_device(): lax.psum_scatter((jnp.dot(sb_mixed, sb_out_w, preferred_element_type=jnp....  51.9 us
    all_gather x1, waiting for transfers between devices, on_device(): lax.all_gather(delta_key_w, 'fs', axis=0, tiled=True)  33.6 us
    all_gather x2, blocking collectives, carried_in(): lax.all_gather(part.astype(kind), axis)  33 us
    all_gather x1, waiting for transfers between devices, on_device(): value_block = lax.all_gather(sb_values, 'sp', axis=0, tiled=True)  26.7 us
    all_gather x1, waiting for transfers between devices, on_device(): key_block = lax.all_gather(sb_keys, 'sp', axis=0, tiled=True)  26.1 us
    all_gather x1, waiting for transfers between devices, on_device(): lax.all_gather(delta_query_w, 'fs', axis=0, tiled=True)  25.7 us
    dot_general x8, matrix products, on_device(): jnp.dot(portion, weight, preferred_element_type=jnp.float32)  23.6 us
    all_gather x1, waiting for transfers between devices, on_device(): lax.all_gather(delta_value_w, 'fs', axis=0, tiled=True)  21.7 us
  transfers between devices with their start and end apart: 10, of which 9 were waited for; matrix products, arithmetic and copies ran while one was open for 28% of the time, Pallas kernels for 0%

commit v1 on v0

--- a/solution.py
+++ b/solution.py
@@ -273,7 +273,12 @@
         usable = jnp.logical_and(shard_first >= 0, shard_first <= own_first)
         return lax.cond(usable, active, inactive, slot_arrays)
 
-    key_block = lax.all_gather(sb_keys, "sp", axis=0, tiled=True)
+    ring = [sb_keys]
+    for hop in range(3):
+        ring.append(lax.ppermute(ring[-1], "sp", [(dev, (dev + 1) % 4) for dev in range(4)]))
+    key_block = jnp.roll(
+        jnp.concatenate(ring[::-1], axis=0), (lax.axis_index("sp") + 1) * ring[0].shape[0], axis=0
+    )
     value_block = lax.all_gather(sb_values, "sp", axis=0, tiled=True)
 
     def per_shard(shard_number, current):

time: 389 us -> 360 us (0.925)
  waiting for transfers between devices: 204 us -> 168 us
    all_gather x1 -> x0, waiting for transfers between devices: 26.1 us -> none  [on_device(): key_block = lax.all_gather(sb_keys, 'sp', axis=0, tiled=True)]
    all_gather x1, waiting for transfers between devices: 26.7 us -> 11.1 us  [on_device(): value_block = lax.all_gather(sb_values, 'sp', axis=0, tiled=True)]
    ppermute x0 -> x3, waiting for transfers between devices: none -> 10.3 us  [on_device(): lax.ppermute(ring[-1], 'sp', [(dev, (dev + 1) % 4) for dev in range(4)])]
    unnamed x40 -> x41, local copies, waits for them, and re-layouts: 5.82 us -> 10.4 us
  transfers between devices with their start and end apart: 10 -> 12, of which waited for: 9 -> 8; matrix products, arithmetic and copies ran while one was open for 28% -> 32% of each run, Pallas kernels for 0% -> 0%
where the time goes in v1:
time: 360 us; the launch traced here: 358 us
  waiting for transfers between devices  168 us (47%)
  matrix products  93.8 us (26%)
  blocking collectives  33.2 us (9%)
  local copies, waits for them, and re-layouts  30 us (8%)
  other arithmetic  16.9 us (5%)
  between operations  13.7 us (4%)
    reduce_scatter x1, waiting for transfers between devices, on_device(): lax.psum_scatter((jnp.dot(sb_mixed, sb_out_w, preferred_element_type=jnp....  51.9 us
    all_gather x1, waiting for transfers between devices, on_device(): lax.all_gather(delta_key_w, 'fs', axis=0, tiled=True)  33.6 us
    all_gather x2, blocking collectives, carried_in(): lax.all_gather(part.astype(kind), axis)  33.2 us
    all_gather x1, waiting for transfers between devices, on_device(): lax.all_gather(delta_query_w, 'fs', axis=0, tiled=True)  25.8 us
    dot_general x8, matrix products, on_device(): jnp.dot(portion, weight, preferred_element_type=jnp.float32)  23.3 us
    all_gather x1, waiting for transfers between devices, on_device(): lax.all_gather(delta_value_w, 'fs', axis=0, tiled=True)  22.5 us
    all_gather x1, waiting for transfers between devices, on_device(): value_block = lax.all_gather(sb_values, 'sp', axis=0, tiled=True)  11.1 us
    unnamed x41, local copies, waits for them, and re-layouts  10.4 us
  transfers between devices with their start and end apart: 12, of which 8 were waited for; matrix products, arithmetic and copies ran while one was open for 32% of the time, Pallas kernels for 0%

profile of v1, /device:TPU:0, one launch (start us, length us, event | category | flops | bytes accessed | tf_op | source)
XLA Modules:
  0.0 358.1 jit_solution(10006473722620727908)
XLA Ops:
  12.1 8.6 %all-gather.26.cloned.1.call-done = bf16[1,256,2048]{2,1,0:T(8,128)(2,1)} async-done(((bf16[1,256,1024]{2,1,0:T(8,128)(2,1)}), bf16[1,256,2048]{2,1,0:T(8,128)(2,1)}) %all-gather.26.cloned.1.call-update) | async-done | bytes 1048592 | tf_op jit(solution)/shard_map/all_gather | solution.py:211
  20.7 1.6 fusion.111
  23.6 1.6 fusion.67
  25.4 33.6 %all-gather.20.cloned.1.call-done = bf16[2048,512]{1,0:T(8,128)(2,1)} async-done(((bf16[512,512]{1,0:T(8,128)(2,1)}), bf16[2048,512]{1,0:T(8,128)(2,1)}) %all-gather.20.cloned.1.call-update) | async-done | bytes 2097168 | tf_op jit(solution)/shard_map/all_gather | solution.py:207
  58.9 3.7 %fusion.116 = (f32[256,512]{1,0:T(8,128)}, f32[256,512]{1,0:T(8,128)}) fusion(bf16[2048,512]{1,0:T(8,128)(2,1)} %all-gather.20.cloned.1.call-done, bf16[1,256,2048]{2,1,0:T(8,128)(2,1)} %all-gather.26.cloned.1.call-done), kind=kOutput, calls=%fused_computation.181 | convolution fusion | flops 537788416 | bytes 4194304 | tf_op jit(solution)/shard_map/dot_general | solution.py:213
  65.5 1.3 fusion.60
  72.0 1.4 convolution_add_fusion.6
  73.5 22.5 %all-gather.22.cloned.1.call-done = bf16[2048,512]{1,0:T(8,128)(2,1)} async-done(((bf16[512,512]{1,0:T(8,128)(2,1)}), bf16[2048,512]{1,0:T(8,128)(2,1)}) %all-gather.22.cloned.1.call-update) | async-done | bytes 2097168 | tf_op jit(solution)/shard_map/all_gather | solution.py:208
  96.0 3.5 divide_multiply_fusion.1
  99.5 2.0 reshape_reshape.3
  101.5 1.9 convolution_add_fusion.5
  103.4 2.1 fusion.78
  105.5 1.6 fusion.82
  107.1 25.8 %all-gather.24.cloned.1.call-done = bf16[2048,512]{1,0:T(8,128)(2,1)} async-done(((bf16[512,512]{1,0:T(8,128)(2,1)}), bf16[2048,512]{1,0:T(8,128)(2,1)}) %all-gather.24.cloned.1.call-update) | async-done | bytes 2097168 | tf_op jit(solution)/shard_map/all_gather | solution.py:206
  132.9 3.9 %fusion.117 = (f32[256,512]{1,0:T(8,128)}, f32[256,512]{1,0:T(8,128)}) fusion(bf16[2048,512]{1,0:T(8,128)(2,1)} %all-gather.24.cloned.1.call-done, bf16[1,256,2048]{2,1,0:T(8,128)(2,1)} %all-gather.26.cloned.1.call-done), kind=kOutput, calls=%fused_computation.182 | convolution fusion | flops 537788416 | bytes 4194304 | tf_op jit(solution)/shard_map/dot_general | solution.py:213
  136.7 2.0 mul.201
  138.8 1.4 reduce_sum.50
  140.3 2.0 reshape.155
  142.3 3.4 convolution_multiply_fusion
  145.7 1.6 bitcast_multiply_fusion.1
  147.3 19.1 %while.57 = (s32[]{:T(128)}, f32[4,128,128]{2,1,0:T(8,128)S(1)}, f32[4,128,128]{2,1,0:T(8,128)S(1)}, f32[4,4]{1,0:T(4,128)S(1)}, f32[4,4,64,128]{3,2,1,0:T(8,128...) while((s32[]{:T(128)}, f32[4,128,128]{2,1,0:T(8,128)S(1)}, ...), condition=%wide.region_12.13_spmd.clone, body=%wide.region_11.12_spmd.clone.sunk | while | flops 252084224 | bytes 3279532 | solution.py:244
  147.3 1.3 convolution_subtract_fusion.7
  148.6 1.5 convolution_add_fusion.14
  150.1 1.5 fusion.213
  153.4 1.5 convolution_add_fusion.14
  154.9 1.5 fusion.213
  156.9 1.3 convolution_subtract_fusion.7
  158.2 1.5 convolution_add_fusion.14
  159.7 1.5 fusion.213
  161.6 1.3 convolution_subtract_fusion.7
  162.9 1.5 convolution_add_fusion.14
  164.4 1.5 fusion.213
  166.4 16.0 %all-gather.1 = bf16[16,128,128]{2,1,0:T(8,128)(2,1)} all-gather(bf16[4,128,128]{2,1,0:T(8,128)(2,1)S(1)} %convert_element_type.96), channel_id=3, replica_groups=mesh['sp'=4,'fs'=4,'tp'=2] {'sp'}, dimensions={0}, use_global_device_ids=true | all-gather | bytes 655360 | tf_op jit(solution)/shard_map/all_gather | solution.py:16
  182.5 17.1 %all-gather.2 = bf16[16,128,128]{2,1,0:T(8,128)(2,1)} all-gather(bf16[4,128,128]{2,1,0:T(8,128)(2,1)S(1)} %convert_element_type.97), channel_id=4, replica_groups=mesh['sp'=4,'fs'=4,'tp'=2] {'sp'}, dimensions={0}, use_global_device_ids=true | all-gather | bytes 655360 | tf_op jit(solution)/shard_map/all_gather | solution.py:16
  199.6 5.2 %while.58 = (s32[]{:T(128)}, f32[4,128,128]{2,1,0:T(8,128)S(1)}, s32[]{:T(128)}, bf16[4,4,128,128]{3,2,1,0:T(8,128)(2,1)}, bf16[4,4,128,128]{3,2,1,0:T(8,128)(2,1)}, /*index=5*/s32[]{:T(128)}, s32[]{:T(128)}) while((s32[]{:T(128)}, f32[4,128,128]{2,1,0:T(8,128)S(1)}, s32[]{:T(128)}, bf16[4,4,128,128]{3,2,1,0:T(8,128)(2,1)}, ...), condition=%wide.region_14.15_spmd.clone, body=%wide.region_13.14_spmd.clone.sunk | while | flops 100990976 | bytes 1575519 | solution.py:33
  204.9 2.6 convolution_convert_fusion.5
  208.5 23.7 %while.56 = (s32[]{:T(128)}, f32[4,128,128]{2,1,0:T(8,128)S(1)}, f32[4,4,64,128]{3,2,1,0:T(8,128)}, f32[4,4]{1,0:T(4,128)S(1)}, f32[4,4,64,128]{3,2,1,0:T(8,128)...) while((s32[]{:T(128)}, f32[4,128,128]{2,1,0:T(8,128)S(1)}, ...), condition=%wide.region_17.18_spmd, body=%wide.region_16.17_spmd.sunk | while | flops 176357376 | bytes 2493593 | solution.py:304
  211.0 1.9 fusion.203
  212.9 1.5 convolution_add_fusion.13
  214.4 1.3 convolution_subtract_fusion.6
  216.9 1.9 fusion.203
  218.8 1.5 convolution_add_fusion.13
  222.8 1.9 fusion.203
  224.7 1.5 convolution_add_fusion.13
  228.7 1.9 fusion.203
  230.7 1.5 convolution_add_fusion.13
  232.2 3.4 convolution_convert_fusion.3
  237.5 2.2 copy.91
  239.6 6.6 %collective-permute-done.1 = bf16[256,512]{1,0:T(8,128)(2,1)} collective-permute-done((bf16[256,512]{1,0:T(8,128)(2,1)}, bf16[256,512]{1,0:T(8,128)(2,1)}, u32[]{:S(2)}, u32[]{:S(2)}) %collective-permute-start.1) | collective-permute-done | bytes 262176 | tf_op jit(solution)/shard_map/ppermute | solution.py:278
  246.3 3.0 convolution_convert_fusion.4
  249.3 1.8 copy.79
  251.1 3.7 %collective-permute-done.2 = bf16[256,512]{1,0:T(8,128)(2,1)} collective-permute-done((bf16[256,512]{1,0:T(8,128)(2,1)}, bf16[256,512]{1,0:T(8,128)(2,1)}, u32[]{:S(2)}, u32[]{:S(2)}) %collective-permute-start.2) | collective-permute-done | bytes 262176 | tf_op jit(solution)/shard_map/ppermute | solution.py:278
  260.7 1.5 copy.80
  262.2 11.1 %all-gather.18.cloned.1.call-done = bf16[1024,512]{1,0:T(8,128)(2,1)} async-done(((bf16[256,512]{1,0:T(8,128)(2,1)}), bf16[1024,512]{1,0:T(8,128)(2,1)}) %all-gather.18.cloned.1.call-update) | async-done | bytes 1048592 | tf_op jit(solution)/shard_map/all_gather | solution.py:282
  273.3 2.3 copy.81
  275.6 1.6 broadcast_in_dim.81
  277.8 14.7 %while.59 = (s32[]{:T(128)}, f32[4,256,8,64]{1,3,2,0:T(8,128)}, f32[4,256,8]{1,2,0:T(8,128)}, s32[]{:T(128)}, bf16[1024,512]{0,1:T(8,128)(2,1)}, /*index=5*/bf16...) while((s32[]{:T(128)}, f32[4,256,8,64]{1,3,2,0:T(8,128)}, ...), condition=%wide.region_6.7_spmd.clone.clone, body=%wide.region_0.6_spmd.clone.clone.sunk | while | flops 218698256 | bytes 25745960 | solution.py:293
  277.8 14.7 %conditional.4 = ((f32[4,256,8,64]{1,3,2,0:T(8,128)}, f32[4,256,8]{1,2,0:T(8,128)})) conditional(s32[]{:T(128)} %convert_element_type.140, (f32[4,256,8,64]{1,3,2,0:T(8,128)}, f32[4,256,8]{1,2,0:T(8,128)}) %tuple.124, (s32[]{:T(128)}, s32[]{:T(128)}, bf16[1024,512]{0,1:T(8,128)(2,1)}, bf16[256,8,64]{0,2,1:T(8,128)(2,1)}, f32[8]{0:T(128)S(1)}, ...), branch_computations={%region_1.1_spmd, %region_2.0_spmd} | conditional | flops 218698256 | bytes 25744700 | solution.py:274
  279.0 2.7 fusion.17
  281.7 5.1 %fusion.13 = f32[8,256,2,128]{1,0,3,2:T(8,128)S(1)} fusion(f32[8,256,2,128]{1,3,2,0:T(8,128)S(1)} %bitcast.258), kind=kOutput, calls=%fused_computation.18 | output fusion | flops 66584576 | bytes 4194304 | tf_op jit(solution)/shard_map/reduce-window.6
  287.7 3.0 fusion.6
  294.2 1.8 multiply_reduce_fusion
  297.9 1.8 fusion.59
  299.6 51.9 %reduce-scatter.2.cloned.1.call-done = bf16[128,2048]{1,0:T(8,128)(2,1)} async-done(((bf16[256,2048]{1,0:T(8,128)(2,1)}), bf16[128,2048]{1,0:T(8,128)(2,1)}) %reduce-scatter.2.cloned.1.call-update) | async-done | bytes 524304 | tf_op jit(solution)/shard_map/reduce_scatter | solution.py:312
  (158 shorter events, 48.1 us)
Async XLA Ops:
  6.5 289.5 %copy-start = (bf16[512,2048]{1,0:T(8,128)(2,1)S(1)}, bf16[512,2048]{1,0:T(8,128)(2,1)}, u32[]{:S(2)}) copy-start(bf16[512,2048]{1,0:T(8,128)(2,1)} %param.40) | copy-start | bytes 6291460
  6.5 4.9 %copy-start.15 = (f32[4]{0:T(128)S(1)}, f32[4]{0:T(128)}, u32[]{:S(2)}) copy-start(f32[4]{0:T(128)} %param.37) | copy-start | bytes 52
  6.5 4.9 %copy-start.14 = (f32[128]{0:T(128)S(1)}, f32[128]{0:T(128)}, u32[]{:S(2)}) copy-start(f32[128]{0:T(128)} %param.39) | copy-start | bytes 1540
  6.5 14.1 %copy-start.8 = (bf16[2048,4]{0,1:T(4,128)(2,1)S(1)}, bf16[2048,4]{0,1:T(4,128)(2,1)}, u32[]{:S(2)}) copy-start(bf16[2048,4]{0,1:T(4,128)(2,1)} %param.34) | copy-start | bytes 49156
  6.5 14.1 %copy-start.12 = (f32[1,4,256]{2,1,0:T(4,128)S(1)}, f32[1,4,256]{2,1,0:T(4,128)}, u32[]{:S(2)}) copy-start(f32[1,4,256]{2,1,0:T(4,128)} %param.38) | copy-start | bytes 12292
  6.5 14.1 %all-gather.26.cloned.1.call-start = ((), (), s32[]{:S(2)}) async-start(), calls=%async_computation.9 | async-start | bytes 1572864 | tf_op jit(solution)/shard_map/all_gather | solution.py:211
  7.3 51.6 %all-gather.20.cloned.1.call-start = ((), (), s32[]{:S(2)}) async-start(), calls=%async_computation.5 | async-start | bytes 2621440 | tf_op jit(solution)/shard_map/all_gather | solution.py:207
  8.0 15.6 %copy-start.9 = (bf16[2048,4]{0,1:T(4,128)(2,1)S(1)}, bf16[2048,4]{0,1:T(4,128)(2,1)}, u32[]{:S(2)}) copy-start(bf16[2048,4]{0,1:T(4,128)(2,1)} %param.35) | copy-start | bytes 49156
  8.0 15.6 %copy-start.13 = (f32[4]{0:T(128)S(1)}, f32[4]{0:T(128)}, u32[]{:S(2)}) copy-start(f32[4]{0:T(128)} %param.36) | copy-start | bytes 52
  8.1 87.9 %all-gather.22.cloned.1.call-start = ((), (), s32[]{:S(2)}) async-start(), calls=%async_computation.6 | async-start | bytes 2621440 | tf_op jit(solution)/shard_map/all_gather | solution.py:208
  8.8 124.1 %all-gather.24.cloned.1.call-start = ((), (), s32[]{:S(2)}) async-start(), calls=%async_computation.7 | async-start | bytes 2621440 | tf_op jit(solution)/shard_map/all_gather | solution.py:206
  9.4 195.5 %all-gather.12.cloned.1.call-start = ((), (), s32[]{:S(2)}) async-start(), calls=%async_computation.1 | async-start | bytes 2621440 | tf_op jit(solution)/shard_map/all_gather | solution.py:204
  10.0 222.3 %all-gather.16.cloned.1.call-start = ((), (), s32[]{:S(2)}) async-start(), calls=%async_computation.3 | async-start | bytes 2621440 | tf_op jit(solution)/shard_map/all_gather | solution.py:205
  10.5 235.7 %all-gather.14.cloned.1.call-start = ((), (), s32[]{:S(2)}) async-start(), calls=%async_computation.2 | async-start | bytes 2621440 | tf_op jit(solution)/shard_map/all_gather | solution.py:203
  11.3 262.0 %all-gather.18.cloned.1.call-start = ((), (), s32[]{:S(2)}) async-start(), calls=%async_computation.4 | async-start | bytes 1310720 | tf_op jit(solution)/shard_map/all_gather | solution.py:282
  65.5 2.6 copy-start.1
  101.5 4.0 %copy-start.5 = (f32[4,64,4,128]{3,2,1,0:T(4,128)S(1)}, f32[4,64,4,128]{3,2,1,0:T(4,128)}, u32[]{:S(2)}) copy-start(f32[4,64,4,128]{3,2,1,0:T(4,128)} %reshape_reshape.3) | copy-start | bytes 1572868
  142.3 3.4 copy-start.2
  142.3 3.4 copy-start.7
  207.5 28.1 %collective-permute-start = (bf16[256,512]{1,0:T(8,128)(2,1)S(1)}, bf16[256,512]{1,0:T(8,128)(2,1)}, u32[]{:S(2)}, u32[]{:S(2)}) collective-permute-start(bf16[256,512]{1,0:T(8,128)(2,1)S(1)} %convolution_convert_fusion.5), channel_id=1, source_target_pairs={{0,8},{8,16},{16,24},{24,0},{1,9},{9,17},{17,25},{25,1},{2,10},{10... | collective-permute-start | bytes 786440 | tf_op jit(solution)/shard_map/ppermute | solution.py:278
  232.2 14.1 %copy-start.3 = (bf16[1,256,2048]{2,1,0:T(8,128)(2,1)S(1)}, bf16[1,256,2048]{2,1,0:T(8,128)(2,1)}, u32[]{:S(2)}) copy-start(bf16[1,256,2048]{2,1,0:T(8,128)(2,1)} %all-gather.26.cloned.1.call-done) | copy-start | bytes 3145732
  235.6 10.6 %collective-permute-start.1 = (bf16[256,512]{1,0:T(8,128)(2,1)}, bf16[256,512]{1,0:T(8,128)(2,1)}, u32[]{:S(2)}, u32[]{:S(2)}) collective-permute-start(bf16[256,512]{1,0:T(8,128)(2,1)} %collective-permute-done), channel_id=1, source_target_pairs={{0,8},{8,16},{16,24},{24,0},{1,9},{9,17},{17,25},{25,1},{2,10},{10... | collective-permute-start | bytes 786440 | tf_op jit(solution)/shard_map/ppermute | solution.py:278
  237.3 114.3 %reduce-scatter.2.cloned.1.call-start = ((), (), s32[]{:S(2)}) async-start(), calls=%async_computation.8 | async-start | bytes 1572864 | tf_op jit(solution)/shard_map/reduce_scatter | solution.py:312
  246.2 8.5 %collective-permute-start.2 = (bf16[256,512]{1,0:T(8,128)(2,1)}, bf16[256,512]{1,0:T(8,128)(2,1)}, u32[]{:S(2)}, u32[]{:S(2)}) collective-permute-start(bf16[256,512]{1,0:T(8,128)(2,1)} %collective-permute-done.1), channel_id=1, source_target_pairs={{0,8},{8,16},{16,24},{24,0},{1,9},{9,17},{17,25},{25,1},{2,10},{10... | collective-permute-start | bytes 786440 | tf_op jit(solution)/shard_map/ppermute | solution.py:278
  262.2 15.5 %copy-start.10 = (f32[8]{0:T(128)S(1)}, f32[8]{0:T(128)}, u32[]{:S(2)}) copy-start(f32[8]{0:T(128)} %param.30) | copy-start | bytes 100
  296.1 1.1 copy-start.4
  296.1 1.8 copy-start.6
  296.1 1.8 copy-start.11
Sparse Core Ops, SparseCore 0:
  8.9 11.7 all-gather.25
  22.5 36.3 all-gather.19
  60.8 35.1 all-gather.21
  97.7 35.1 all-gather.23
  134.6 35.1 all-gather.11
  171.5 35.1 all-gather.15
  208.5 35.1 all-gather.13
  245.3 27.9 all-gather.17
  299.8 51.7 reduce-scatter.1
